TPU v7x, 256 devices: a 4x2x16 block of a 4x16x16 slice. The times are simulated.
256 devices in a mesh: grp: 2 (over y), fs: 32 (over z, core), tp: 4 (over x).
Axes of the slice: x: 4, y: 2, z: 16, core: 2. Of those that a mesh axis runs over, the one named last changes fastest.
The devices are a block of a 4x16x16 slice.
Arguments:
- tokens: bfloat16 [1536, 2048], P(('grp', 'tp')), parts along dimension 0, may hold values from -6 to 6
- norm_gain: float32 [2048], P('fs'), may hold values from 0.1 to 1.9
- up_trained: float32 [2048, 8192], P('fs', 'tp'), may hold values from -0.125 to 0.125
- down_trained: float32 [2048, 8192], P('fs', 'tp'), may hold values from -0.125 to 0.125
Outputs:
- up_serving: bfloat16 [4096, 8192], P('grp', 'fs'), parts along dimension 0
- down_serving: bfloat16 [4096, 8192], P('grp', 'fs'), parts along dimension 0
- prompt_output: bfloat16 [1536, 2048], P(('grp', 'tp'), 'fs'), parts along dimension 0
There are 2 independent parts, one for each index of `grp`. A program takes and returns all parts, laid end to end along the dimension named above; an argument that names none is the same for every part. Nothing has to cross between parts.
All inputs are finite; a program needn't handle non-finite values.
Results may differ from a plain program's by a relative error of at most 0.0074.
Values may be sent and summed in bfloat16 or wider, within the bound.
A program may use at most 64 MiB of HBM per device.

v0:
```python
import jax
import jax.numpy as jnp
from jax import lax
from jax.sharding import PartitionSpec as P

epsilon = 1e-06


def joined_along(parts, dim):
    parts = jnp.moveaxis(parts, 0, dim)
    dims = parts.shape
    return parts.reshape(*dims[:dim], dims[dim] * dims[dim + 1], *dims[dim + 2 :])


def copy_for_each(x, axis):
    devices = lax.axis_size(axis)
    return lax.all_to_all(jnp.broadcast_to(x[None], (devices, *x.shape)), axis, 0, 0, tiled=True)


def collect(x, axis, dim):
    return joined_along(copy_for_each(x, axis), dim)


def in_blocks(x, dim, devices):
    dims = x.shape
    parts = x.reshape(*dims[:dim], devices, dims[dim] // devices, *dims[dim + 1 :])
    return jnp.moveaxis(parts, dim, 0)


def sum_at_owner(x, axis, dim):
    parts = in_blocks(x, dim, lax.axis_size(axis))
    arrived = lax.all_to_all(parts, axis, split_axis=0, concat_axis=0, tiled=True)
    return arrived.astype(jnp.float32).sum(axis=0)


def local(tokens, norm_gain, up_trained, down_trained):
    shards = lax.axis_size("fs")
    groups = lax.axis_size("tp")
    rows_local = up_trained.shape[0]
    cols_local = up_trained.shape[1]
    folded = (norm_gain[:, None] * up_trained).astype(jnp.bfloat16)
    stacked = jnp.stack([folded, down_trained.astype(jnp.bfloat16)])
    served_width = cols_local * groups // shards
    blocks_here = cols_local // served_width
    quarter_rows = rows_local // groups
    pieces = stacked.reshape(2, groups, quarter_rows, blocks_here, served_width)
    moved = lax.all_to_all(pieces, "tp", split_axis=1, concat_axis=3, tiled=True)
    placed = lax.all_to_all(moved, "fs", split_axis=3, concat_axis=2, tiled=True)
    ordered = placed.reshape(2, shards, quarter_rows, served_width)
    joined = collect(ordered, "tp", 2)
    owned = joined.reshape(2, rows_local * shards, served_width)
    up_serving = owned[0]
    down_serving = owned[1]
    values = tokens.astype(jnp.float32)
    scale = lax.rsqrt(jnp.mean(values * values, axis=1, keepdims=True) + epsilon)
    normed = (values * scale).astype(jnp.bfloat16)
    hidden = jnp.dot(normed, up_serving, preferred_element_type=jnp.float32)
    active = jnp.square(jax.nn.relu(hidden)).astype(jnp.bfloat16)
    summed = sum_at_owner(
        lax.dot_general(
            down_serving, active, (((1,), (1,)), ((), ())), preferred_element_type=jnp.float32
        ).astype(jnp.bfloat16),
        "fs",
        0,
    )
    prompt_output = summed.T.astype(jnp.bfloat16)
    return (up_serving, down_serving, prompt_output)


def solution(mesh):
    in_specs = (P(("grp", "tp"), None), P("fs"), P("fs", "tp"), P("fs", "tp"))
    out_specs = (P("grp", "fs"), P("grp", "fs"), P(("grp", "tp"), "fs"))
    return jax.shard_map(local, mesh=mesh, in_specs=in_specs, out_specs=out_specs, check_vma=False)
```

profile of v0, /device:TPU:33, one launch (start us, length us, event | category | flops | bytes accessed | tf_op | source)
XLA Modules:
  0.0 171.2 jit_solution(14890770866300171647)
XLA Ops:
  0.6 0.0 copy-start.3
  0.6 1.2 multiply_convert_fusion
  1.8 0.1 copy.23
  1.9 0.0 copy-done.3
  2.0 0.1 copy.24
  2.0 0.1 pad_maximum_fusion
  2.1 11.9 %all_to_all.43 = bf16[2,4,16,8,256]{4,3,2,0,1:T(8,128)(2,1)S(1)} all-to-all(bf16[2,4,16,8,256]{4,3,2,0,1:T(8,128)(2,1)S(1)} %copy.17), channel_id=1, replica_groups=mesh['grp'=2,'fs'=32,'tp'=4] {'tp'}, dimensions={1} | all-to-all | bytes 1048576 | tf_op jit(solution)/shard_map/all_to_all | solution.py:47
  14.0 0.1 copy.28
  14.0 0.3 copy.19
  14.3 60.6 %all_to_all.44 = bf16[2,1,16,32,256]{4,2,0,1,3:T(8,128)(2,1)S(1)} all-to-all(bf16[2,1,16,32,256]{4,2,0,1,3:T(8,128)(2,1)S(1)} %copy.19), channel_id=1, replica_groups=mesh['grp'=2,'fs'=32,'tp'=4] {'fs'}, dimensions={3} | all-to-all | bytes 1048576 | tf_op jit(solution)/shard_map/all_to_all | solution.py:48
  75.0 1.5 broadcast_in_dim.10
  76.5 0.0 copy-start.2
  76.5 3.8 %all-to-all-start.2 = ((bf16[4,2,32,16,256]{4,3,2,1,0:T(8,128)(2,1)}), bf16[4,2,32,16,256]{4,3,2,1,0:T(8,128)(2,1)S(1)}, u32[]{:S(2)}, u32[]{:S(2)}) async-start(bf16[4,2,32,16,256]{4,3,2,1,0:T(8,128)(2,1)} %broadcast_in_dim.10), calls=%async_computation.2 | async-start | bytes 4194304 | tf_op jit(solution)/shard_map/all_to_all | solution.py:17
  80.4 0.0 copy-done.2
  80.4 0.2 fusion
  80.6 25.6 %all-to-all-done.2 = bf16[4,2,32,16,256]{4,3,2,1,0:T(8,128)(2,1)S(1)} async-done(((bf16[4,2,32,16,256]{4,3,2,1,0:T(8,128)(2,1)}), bf16[4,2,32,16,256]{4,3,2,1,0:T(8,128)(2,1)S(1)}, u32[]{:S(2)}, u32[]{:S(2)}) %all-to-all-start.2) | async-done | bytes 2097184 | tf_op jit(solution)/shard_map/all_to_all | solution.py:17
  106.2 0.3 copy.27
  106.5 0.2 fusion.10
  106.8 0.0 copy-start.1
  106.8 0.0 copy-start
  106.8 0.9 copy-done.1
  107.7 2.3 %convolution_convert_fusion = bf16[2048,192]{0,1:T(8,128)(2,1)S(1)} fusion(bf16[2048,256]{1,0:T(8,128)(2,1)S(1)} %bitcast.29, bf16[2048,256]{1,0:T(8,128)(2,1)S(1)} %bitcast.31, bf16[192,2048]{1,0:T(8,128)(2,1)} %param.4, f32[192]{0:T(256)S(1)} %add_rsqrt_fusion), kind=kOutput, calls=%fused_computation | convolution fusion | flops 404373504 | bytes 3670784 | tf_op jit(solution)/shard_map/dot_general | solution.py:60
  110.0 0.0 copy-done
  110.0 0.5 copy.22
  110.5 59.9 %all_to_all.45 = bf16[32,64,192]{2,1,0:T(8,128)(2,1)S(1)} all-to-all(bf16[32,64,192]{2,1,0:T(8,128)(2,1)S(1)} %bitcast.28), channel_id=1, replica_groups=mesh['grp'=2,'fs'=32,'tp'=4] {'fs'}, dimensions={0} | all-to-all | bytes 1572864 | tf_op jit(solution)/shard_map/all_to_all | solution.py:32
  170.4 0.8 reduce_sum.22
  (4 shorter events, 0.1 us)
Async XLA Ops:
  0.6 1.3 copy-start.3
  76.5 3.8 %copy-start.2 = (bf16[192,2048]{1,0:T(8,128)(2,1)S(1)}, bf16[192,2048]{1,0:T(8,128)(2,1)}, u32[]{:S(2)}) copy-start(bf16[192,2048]{1,0:T(8,128)(2,1)} %param.4) | copy-start | bytes 2359300
  76.5 29.7 %all-to-all-start.2 = ((bf16[4,2,32,16,256]{4,3,2,1,0:T(8,128)(2,1)}), bf16[4,2,32,16,256]{4,3,2,1,0:T(8,128)(2,1)S(1)}, u32[]{:S(2)}, u32[]{:S(2)}) async-start(bf16[4,2,32,16,256]{4,3,2,1,0:T(8,128)(2,1)} %broadcast_in_dim.10), calls=%async_computation.2 | async-start | bytes 4194304 | tf_op jit(solution)/shard_map/all_to_all | solution.py:17
  106.8 1.0 copy-start.1
  106.8 3.3 %copy-start = (bf16[1,32,4,16,256]{4,3,2,1,0:T(8,128)(2,1)}, bf16[1,32,4,16,256]{4,3,2,1,0:T(8,128)(2,1)S(1)}, u32[]{:S(2)}) copy-start(bf16[1,32,4,16,256]{4,3,2,1,0:T(8,128)(2,1)S(1)} %get-tuple-element.3) | copy-start | bytes 3145732
where the time goes:
time: 172 us; the launch traced here: 171 us
  blocking collectives  132 us (77%)
  waiting for transfers between devices  25.6 us (15%)
  local copies, waits for them, and re-layouts  4.06 us (2%)
  starting transfers between devices  3.83 us (2%)
  other arithmetic  2.33 us (1%)
  matrix products  2.28 us (1%)
    all_to_all x1, blocking collectives, local(): lax.all_to_all(moved, 'fs', split_axis=3, concat_axis=2, tiled=True)  60.6 us
    all_to_all x1, blocking collectives, sum_at_owner(): lax.all_to_all(parts, axis, split_axis=0, concat_axis=0, tiled=True)  59.9 us
    all_to_all x1, waiting for transfers between devices, copy_for_each(): lax.all_to_all(jnp.broadcast_to(x[None], (devices, *x.shape)), axis, 0, 0...  25.6 us
    all_to_all x1, blocking collectives, local(): lax.all_to_all(pieces, 'tp', split_axis=1, concat_axis=3, tiled=True)  11.9 us
    all_to_all x1, starting transfers between devices, copy_for_each(): lax.all_to_all(jnp.broadcast_to(x[None], (devices, *x.shape)), axis, 0, 0...  3.83 us
  transfers between devices with their start and end apart: 1, of which 1 were waited for; matrix products, arithmetic and copies ran while one was open for 0% of the time, Pallas kernels for 0%

commit v1 on v0

v1 whole, which is shorter than its diff:
```python
import functools

import jax
import jax.numpy as jnp
from jax import lax
from jax.experimental import pallas as pl
from jax.experimental.pallas import tpu as pltpu
from jax.sharding import PartitionSpec as P

MESH = pl.DeviceIdType.MESH
epsilon = 1e-06


def ring_order(n):
    half = n // 2
    pairs = [d for d in range(half - 1, 5, -1)] + [4, 3, 1, 5, 2]
    slots = [half]
    first = {}
    for d in pairs:
        first[d] = len(slots)
        slots += [d, n - d]
    slots.append(0)
    return slots, first


def kernel(
    shards,
    planes,
    tok_hbm,
    gain_hbm,
    up_hbm,
    down_hbm,
    up_out,
    down_out,
    y_ref,
    tok,
    gain,
    raw,
    normed,
    src,
    relay,
    full,
    mine,
    give,
    got,
    sums,
    stage,
    final,
    in_sem,
    out_sem,
    p1_send,
    p1_recv,
    p2_send,
    full_recv,
    p3_send,
    p4_send,
    pair_send,
    pair_recv,
    sum_send,
    stage_recv,
    final_recv,
):
    f = lax.axis_index("fs")
    x = lax.axis_index("tp")
    n_z = shards // 2
    z = f // 2
    c = f % 2
    rows, width = full.shape[2], full.shape[3]
    per_plane = src.shape[2]
    blocks_here = planes * per_plane
    sources = shards // planes

    barrier = pltpu.get_barrier_semaphore()
    for step in range(1, planes):
        pl.semaphore_signal(barrier, inc=1, device_id={"tp": (x + step) % planes}, device_id_type=MESH)

    def greet(step, carry):
        pl.semaphore_signal(barrier, inc=1, device_id={"fs": (f + step) % shards}, device_id_type=MESH)
        return carry

    lax.fori_loop(1, shards, greet, 0)

    loads = [
        pltpu.make_async_copy(gain_hbm, gain, in_sem.at[0]),
        pltpu.make_async_copy(up_hbm, raw.at[0], in_sem.at[1]),
        pltpu.make_async_copy(down_hbm, raw.at[1], in_sem.at[2]),
        pltpu.make_async_copy(tok_hbm, tok, in_sem.at[3]),
    ]
    for load in loads:
        load.start()

    def first_block(plane):
        return (plane + 4 * planes - z - 2 * c + shards * planes) % planes

    loads[0].wait()
    row_at = lax.broadcasted_iota(jnp.int32, (rows, rows), 0)
    col_at = lax.broadcasted_iota(jnp.int32, (rows, rows), 1)
    column = jnp.sum(
        jnp.where(row_at == col_at, jnp.broadcast_to(gain[...], (rows, rows)), 0.0), axis=1, keepdims=True
    )
    for kind in range(2):
        loads[1 + kind].wait()
        for plane in range(planes):
            for b in range(per_plane):
                at = pl.multiple_of((planes * b + first_block(plane)) * width, width)
                block = raw[kind, :, pl.ds(at, width)]
                if kind == 0:
                    block = block * column
                src[kind, plane, b] = block.astype(jnp.bfloat16)
    loads[3].wait()
    step_rows = 64
    for r in range(0, tok.shape[0], step_rows):
        values = tok[r : r + step_rows, :].astype(jnp.float32)
        scale = lax.rsqrt(jnp.mean(values * values, axis=1, keepdims=True) + epsilon)
        normed[r : r + step_rows, :] = (values * scale).astype(jnp.bfloat16)

    pl.semaphore_wait(barrier, planes - 1 + shards - 1)

    pending = []

    for kind in range(2):
        for step in (1, 3, 2):
            plane = (x + step) % planes
            copy = pltpu.make_async_remote_copy(
                src_ref=src.at[kind, plane],
                dst_ref=relay.at[kind, x],
                send_sem=p1_send.at[kind, step - 1],
                recv_sem=p1_recv.at[kind, x],
                device_id={"tp": plane},
                device_id_type=MESH,
            )
            copy.start()
            pending.append((None, copy))

    s = first_block(x)
    for kind in range(2):
        for step in (0, 3, 1, 2):
            a = (x + step) % planes
            if step == 0:
                held = src.at[kind, x]
            else:
                held = relay.at[kind, a]
                pltpu.make_async_copy(src.at[kind, 0], held, p1_recv.at[kind, a]).wait()
            for b in range(per_plane):
                to = blocks_here * a + planes * b + s
                away = to != f
                copy = pltpu.make_async_remote_copy(
                    src_ref=held.at[b],
                    dst_ref=full.at[kind, f],
                    send_sem=p2_send.at[kind, step * per_plane + b],
                    recv_sem=full_recv.at[kind, f],
                    device_id={"fs": to},
                    device_id_type=MESH,
                )
                pl.when(away)(copy.start)
                pending.append((away, copy))

                @pl.when(jnp.logical_not(away))
                def _():
                    full[kind, f] = held[b]

    def source(plane, i):
        r = (plane + 2 * shards - f) % planes
        odd = (z + r) % 2
        near = (i + 1) // 2
        even_at = jnp.int32(2 * near if i % 2 else n_z - 2 * near)
        odd_at = jnp.int32(1 + 2 * (i // 2) if i % 2 == 0 else n_z - 1 - 2 * (i // 2))
        zs = (z + jnp.where(odd == 1, odd_at, even_at)) % n_z
        return 2 * zs + ((zs + planes - r) // 2) % 2

    def arrived(kind, at):
        return pltpu.make_async_copy(full.at[kind, at], full.at[kind, at], full_recv.at[kind, at])

    def forward(kind, at, step, sem):
        copy = pltpu.make_async_remote_copy(
            src_ref=full.at[kind, at],
            dst_ref=full.at[kind, at],
            send_sem=sem,
            recv_sem=full_recv.at[kind, at],
            device_id={"tp": (x + step) % planes},
            device_id_type=MESH,
        )
        copy.start()
        pending.append((None, copy))

    def collect(kind):
        for i in range(sources):
            at = source(x, i)
            pl.when(at != f)(arrived(kind, at).wait)
            forward(kind, at, 1, p3_send.at[kind, i, 0])
            forward(kind, at, 3, p3_send.at[kind, i, 1])
        for i in range(sources):
            for step, parity in ((3, 0), (1, 1)):
                at = source((x + step) % planes, i)
                arrived(kind, at).wait()
                if i % 2 == parity:
                    forward(kind, at, 4 - step, p4_send.at[kind, i])
        for i in range(sources):
            arrived(kind, source((x + 2) % planes, i)).wait()

    collect(0)
    put_up = pltpu.make_async_copy(full.at[0], up_out, out_sem.at[0])
    put_up.start()
    up = full[0].reshape(shards * rows, width)
    hidden = jnp.dot(normed[...], up, preferred_element_type=jnp.float32)
    active = jnp.square(jnp.maximum(hidden, 0.0)).astype(jnp.bfloat16)

    collect(1)
    put_down = pltpu.make_async_copy(full.at[1], down_out, out_sem.at[1])
    put_down.start()

    half = tok.shape[0] // 2
    low = lax.broadcasted_iota(jnp.int32, (half, 2 * rows), 1) < rows
    slots, first = ring_order(n_z)
    for slot, ahead in enumerate(slots):
        owner = (z + ahead) % n_z
        block = full[1, pl.ds(2 * owner, 2)].reshape(2 * rows, width)
        part = lax.dot_general(active, block, (((1,), (1,)), ((), ())), preferred_element_type=jnp.float32)
        top, bottom = part[:half], part[half:]
        even = jnp.where(low, top, pltpu.roll(bottom, rows, 1))
        odd = jnp.where(low, pltpu.roll(top, rows, 1), bottom)
        mine[slot] = jnp.where(c == 0, even, odd)
        give[slot] = jnp.where(c == 0, odd, even).astype(jnp.bfloat16)

    cut = first[1]
    pair = []
    for j, (start, stop) in enumerate(((0, cut), (cut, n_z))):
        copy = pltpu.make_async_remote_copy(
            src_ref=give.at[pl.ds(start, stop - start)],
            dst_ref=got.at[pl.ds(start, stop - start)],
            send_sem=pair_send.at[j],
            recv_sem=pair_recv.at[j],
            device_id={"fs": f + 1 - 2 * c},
            device_id_type=MESH,
        )
        copy.start()
        pair.append(copy)

    top_d = n_z // 2
    groups = [(5, list(range(6, top_d + 1)), list(range(6, top_d))), (2, [3, 4], [3, 4])]
    sign = 1 - 2 * c

    def place(side, d):
        if d == top_d:
            return 0
        return first[d] + (c if side == 0 else 1 - c)

    def toward(side, d):
        return (z + n_z + (sign if side == 0 else -sign) * d) % n_z

    def pass_on(slot, dst, recv, to_z, j):
        copy = pltpu.make_async_remote_copy(
            src_ref=sums.at[slot],
            dst_ref=dst,
            send_sem=sum_send.at[j],
            recv_sem=recv,
            device_id={"fs": 2 * to_z + c},
            device_id_type=MESH,
        )
        copy.start()
        pending.append((None, copy))

    pair[0].wait_recv()
    for slot in range(cut):
        sums[slot] = (mine[slot] + got[slot].astype(jnp.float32)).astype(jnp.bfloat16)
    order = []
    for agent, big, small in groups:
        for side, members in ((0, big), (1, small)):
            for d in members:
                order.append((d - agent, d, side, agent))
    stage_at = {}
    count = 0
    for _, d, side, agent in sorted(order, reverse=True):
        stage_at[(side, d)] = count
        pass_on(place(side, d), stage.at[count], stage_recv.at[count], toward(side, d - agent), count)
        count += 1

    pair[1].wait_recv()
    for side in range(2):
        slot = place(side, 1)
        sums[slot] = (mine[slot] + got[slot].astype(jnp.float32)).astype(jnp.bfloat16)
    for side in range(2):
        pass_on(place(side, 1), final.at[4 + side], final_recv.at[4 + side], toward(side, 1), count + 4 + side)
    for g, (agent, big, small) in enumerate(groups):
        for side, members in ((0, big), (1, small)):
            slot = place(side, agent)
            total = mine[slot] + got[slot].astype(jnp.float32)
            for d in members:
                j = stage_at[(side, d)]
                pltpu.make_async_copy(stage.at[j], stage.at[j], stage_recv.at[j]).wait()
                total = total + stage[j].astype(jnp.float32)
            sums[slot] = total.astype(jnp.bfloat16)
            k = 2 * g + side
            pass_on(slot, final.at[k], final_recv.at[k], toward(side, agent), count + k)
    own = n_z - 1
    total = mine[own] + got[own].astype(jnp.float32)
    for k in (4, 5, 2, 3, 0, 1):
        pltpu.make_async_copy(final.at[k], final.at[k], final_recv.at[k]).wait()
        total = total + final[k].astype(jnp.float32)
    total = total.astype(jnp.bfloat16)
    y_ref[0:half, :] = total[:, 0:rows]
    y_ref[half : 2 * half, :] = total[:, rows : 2 * rows]

    put_up.wait()
    put_down.wait()
    for copy in pair:
        copy.wait_send()
    for when, copy in pending:
        if when is None:
            copy.wait_send()
        else:
            pl.when(when)(copy.wait_send)


def local(shards, planes, tokens, norm_gain, up_trained, down_trained):
    rows, cols = up_trained.shape
    count, depth = tokens.shape
    width = cols * planes // shards
    per_plane = cols // width // planes
    n_z = shards // 2
    half = count // 2
    bf16, f32 = jnp.bfloat16, jnp.float32
    served = jax.ShapeDtypeStruct((shards, rows, width), bf16)
    dma = pltpu.SemaphoreType.DMA
    any_space = pl.BlockSpec(memory_space=pl.ANY)
    up, down, y = pl.pallas_call(
        functools.partial(kernel, shards, planes),
        out_shape=(served, served, jax.ShapeDtypeStruct((count, rows), bf16)),
        in_specs=[any_space] * 4,
        out_specs=(any_space, any_space, pl.BlockSpec(memory_space=pltpu.VMEM)),
        scratch_shapes=[
            pltpu.VMEM((count, depth), bf16),
            pltpu.VMEM((1, rows), f32),
            pltpu.VMEM((2, rows, cols), f32),
            pltpu.VMEM((count, depth), bf16),
            pltpu.VMEM((2, planes, per_plane, rows, width), bf16),
            pltpu.VMEM((2, planes, per_plane, rows, width), bf16),
            pltpu.VMEM((2, shards, rows, width), bf16),
            pltpu.VMEM((n_z, half, 2 * rows), f32),
            pltpu.VMEM((n_z, half, 2 * rows), bf16),
            pltpu.VMEM((n_z, half, 2 * rows), bf16),
            pltpu.VMEM((n_z, half, 2 * rows), bf16),
            pltpu.VMEM((n_z, half, 2 * rows), bf16),
            pltpu.VMEM((6, half, 2 * rows), bf16),
            dma((4,)),
            dma((2,)),
            dma((2, planes - 1)),
            dma((2, planes)),
            dma((2, planes * per_plane)),
            dma((2, shards)),
            dma((2, shards // planes, 2)),
            dma((2, shards // planes)),
            dma((2,)),
            dma((2,)),
            dma((n_z,)),
            dma((n_z,)),
            dma((6,)),
        ],
        compiler_params=pltpu.CompilerParams(
            collective_id=0, has_side_effects=True, vmem_limit_bytes=48 * 1024 * 1024
        ),
        name="handoff",
    )(tokens, norm_gain.reshape(1, rows), up_trained, down_trained)
    return (up.reshape(shards * rows, width), down.reshape(shards * rows, width), y)


def solution(mesh):
    in_specs = (P(("grp", "tp"), None), P("fs"), P("fs", "tp"), P("fs", "tp"))
    out_specs = (P("grp", "fs"), P("grp", "fs"), P(("grp", "tp"), "fs"))
    body = functools.partial(local, mesh.shape["fs"], mesh.shape["tp"])
    return jax.shard_map(body, mesh=mesh, in_specs=in_specs, out_specs=out_specs, check_vma=False)
```

time: 172 us -> 91.2 us (0.53)
  blocking collectives: 132 us -> 0 us
  Pallas kernels: 0 us -> 83.3 us
  waiting for transfers between devices: 25.6 us -> 0 us
  starting transfers between devices: 3.83 us -> 0 us
  local copies, waits for them, and re-layouts: 4.06 us -> 6.51 us
  other arithmetic: 2.33 us -> 0 us
  matrix products: 2.28 us -> 0 us
    all_to_all x3 -> x0, blocking collectives: 132 us -> none  [the longest x1 60.6 us: local(): lax.all_to_all(moved, 'fs', split_axis=3, concat_axis=2, tiled=True)]
    pallas_call x0 -> x1, Pallas kernels: none -> 83.3 us  [local(): pl.pallas_call(functools.partial(kernel, shards, planes), out_shape=(serv...]
    all_to_all x1 -> x0, waiting for transfers between devices: 25.6 us -> none  [copy_for_each(): lax.all_to_all(jnp.broadcast_to(x[None], (devices, *x.shape)), axis, 0, 0...]
    unnamed x10 -> x11, local copies, waits for them, and re-layouts: 1.07 us -> 6.51 us
    all_to_all x1 -> x0, starting transfers between devices: 3.83 us -> none  [copy_for_each(): lax.all_to_all(jnp.broadcast_to(x[None], (devices, *x.shape)), axis, 0, 0...]
    dot_general x1 -> x0, matrix products: 2.28 us -> none  [local(): lax.dot_general(down_serving, active, (((1,), (1,)), ((), ())), preferred...]
  transfers between devices with their start and end apart: 1 -> 0, of which waited for: 1 -> 0; matrix products, arithmetic and copies ran while one was open for 0% -> 0% of each run, Pallas kernels for 0% -> 0%
where the time goes in v1:
time: 91.2 us; the launch traced here: 90.4 us
  Pallas kernels  83.3 us (91%)
  local copies, waits for them, and re-layouts  6.51 us (7%)
    pallas_call x1, Pallas kernels, local(): pl.pallas_call(functools.partial(kernel, shards, planes), out_shape=(serv...  83.3 us
    unnamed x11, local copies, waits for them, and re-layouts  6.51 us

profile of v1, /device:TPU:33, one launch (start us, length us, event | category | flops | bytes accessed | tf_op | source)
XLA Modules:
  0.0 90.4 jit_solution(1893996321448214224)
XLA Ops:
  0.6 0.0 copy-start.3
  0.6 0.6 copy-done.3
  1.3 0.0 copy-start
  1.3 1.1 %copy-done = bf16[192,2048]{1,0:T(8,128)(2,1)S(1)} copy-done((bf16[192,2048]{1,0:T(8,128)(2,1)S(1)}, bf16[192,2048]{1,0:T(8,128)(2,1)}, u32[]{:S(2)}) %copy-start) | copy-done | bytes 786456
  2.4 0.0 copy-start.1
  2.4 1.0 %copy-done.1 = f32[64,2048]{1,0:T(8,128)S(1)} copy-done((f32[64,2048]{1,0:T(8,128)S(1)}, f32[64,2048]{1,0:T(8,128)}, u32[]{:S(2)}) %copy-start.1) | copy-done | bytes 524312
  3.5 0.0 copy-start.2
  3.5 1.0 %copy-done.2 = f32[64,2048]{1,0:T(8,128)S(1)} copy-done((f32[64,2048]{1,0:T(8,128)S(1)}, f32[64,2048]{1,0:T(8,128)}, u32[]{:S(2)}) %copy-start.2) | copy-done | bytes 524312
  4.5 83.3 %handoff.1 = (bf16[32,64,256]{2,1,0:T(8,128)(2,1)S(1)}, bf16[32,64,256]{2,1,0:T(8,128)(2,1)S(1)}, bf16[192,64]{1,0:T(8,128)(2,1)S(1)}) custom-call(bf16[192,2048]{1,0:T(8,128)(2,1)S(1)} %copy-done, f32[1,64]{1,0:T(1,128)S(1)} %bitcast.5, f32[64,2048]{1,0:T(8,128)S(1)} %copy-done.1, f32[64,2048]{1,0:T(8,128)S(1)} %copy-done.2), custom_call_target="tpu_custom_call" | custom-call | tf_op jit(solution)/shard_map/handoff/pallas_call | solution.py:326
  87.8 0.7 copy.7
  88.5 1.0 %copy.10 = bf16[2048,256]{1,0:T(8,128)(2,1)} copy(bf16[2048,256]{1,0:T(8,128)(2,1)S(1)} %bitcast.4) | data formatting | bytes 2097152
  89.5 1.0 %copy.11 = bf16[2048,256]{1,0:T(8,128)(2,1)} copy(bf16[2048,256]{1,0:T(8,128)(2,1)S(1)} %bitcast.3) | data formatting | bytes 2097152
Async XLA Ops:
  0.6 0.7 copy-start.3
  1.3 1.1 %copy-start = (bf16[192,2048]{1,0:T(8,128)(2,1)S(1)}, bf16[192,2048]{1,0:T(8,128)(2,1)}, u32[]{:S(2)}) copy-start(bf16[192,2048]{1,0:T(8,128)(2,1)} %tok_hbm.1) | copy-start | bytes 2359300
  2.4 1.0 %copy-start.1 = (f32[64,2048]{1,0:T(8,128)S(1)}, f32[64,2048]{1,0:T(8,128)}, u32[]{:S(2)}) copy-start(f32[64,2048]{1,0:T(8,128)} %up_hbm.1) | copy-start | bytes 1572868
  3.5 1.0 %copy-start.2 = (f32[64,2048]{1,0:T(8,128)S(1)}, f32[64,2048]{1,0:T(8,128)}, u32[]{:S(2)}) copy-start(f32[64,2048]{1,0:T(8,128)} %down_hbm.1) | copy-start | bytes 1572868

commit v2 on v1

--- a/solution.py
+++ b/solution.py
@@ -9,6 +9,7 @@
 
 MESH = pl.DeviceIdType.MESH
 epsilon = 1e-06
+ahead_by = 5
 
 
 def ring_order(n):
@@ -59,6 +60,8 @@
     sum_send,
     stage_recv,
     final_recv,
+    token,
+    ready,
 ):
     f = lax.axis_index("fs")
     x = lax.axis_index("tp")
@@ -70,15 +73,19 @@
     blocks_here = planes * per_plane
     sources = shards // planes
 
+    last = n_z - 1
     barrier = pltpu.get_barrier_semaphore()
     for step in range(1, planes):
         pl.semaphore_signal(barrier, inc=1, device_id={"tp": (x + step) % planes}, device_id_type=MESH)
-
-    def greet(step, carry):
-        pl.semaphore_signal(barrier, inc=1, device_id={"fs": (f + step) % shards}, device_id_type=MESH)
-        return carry
-
-    lax.fori_loop(1, shards, greet, 0)
+    pl.semaphore_signal(barrier, inc=1, device_id={"fs": f + 1 - 2 * c}, device_id_type=MESH)
+
+    @pl.when(z > 0)
+    def _():
+        pl.semaphore_signal(barrier, inc=1, device_id={"fs": f - 2}, device_id_type=MESH)
+
+    @pl.when(z < last)
+    def _():
+        pl.semaphore_signal(barrier, inc=1, device_id={"fs": f + 2}, device_id_type=MESH)
 
     loads = [
         pltpu.make_async_copy(gain_hbm, gain, in_sem.at[0]),
@@ -107,6 +114,7 @@
                 if kind == 0:
                     block = block * column
                 src[kind, plane, b] = block.astype(jnp.bfloat16)
+        relay[kind, x] = src[kind, x]
     loads[3].wait()
     step_rows = 64
     for r in range(0, tok.shape[0], step_rows):
@@ -114,65 +122,85 @@
         scale = lax.rsqrt(jnp.mean(values * values, axis=1, keepdims=True) + epsilon)
         normed[r : r + step_rows, :] = (values * scale).astype(jnp.bfloat16)
 
-    pl.semaphore_wait(barrier, planes - 1 + shards - 1)
-
-    pending = []
+    pl.semaphore_wait(barrier, planes + jnp.where(z > 0, 1, 0) + jnp.where(z < last, 1, 0))
+
+    def spread(kind, step):
+        plane = (x + step) % planes
+        return pltpu.make_async_remote_copy(
+            src_ref=src.at[kind, plane],
+            dst_ref=relay.at[kind, x],
+            send_sem=p1_send.at[kind, step - 1],
+            recv_sem=p1_recv.at[kind, x],
+            device_id={"tp": plane},
+            device_id_type=MESH,
+        )
 
     for kind in range(2):
         for step in (1, 3, 2):
-            plane = (x + step) % planes
-            copy = pltpu.make_async_remote_copy(
-                src_ref=src.at[kind, plane],
-                dst_ref=relay.at[kind, x],
-                send_sem=p1_send.at[kind, step - 1],
-                recv_sem=p1_recv.at[kind, x],
-                device_id={"tp": plane},
-                device_id_type=MESH,
-            )
-            copy.start()
-            pending.append((None, copy))
-
-    s = first_block(x)
-    for kind in range(2):
-        for step in (0, 3, 1, 2):
-            a = (x + step) % planes
-            if step == 0:
-                held = src.at[kind, x]
-            else:
-                held = relay.at[kind, a]
-                pltpu.make_async_copy(src.at[kind, 0], held, p1_recv.at[kind, a]).wait()
-            for b in range(per_plane):
-                to = blocks_here * a + planes * b + s
-                away = to != f
-                copy = pltpu.make_async_remote_copy(
-                    src_ref=held.at[b],
-                    dst_ref=full.at[kind, f],
-                    send_sem=p2_send.at[kind, step * per_plane + b],
-                    recv_sem=full_recv.at[kind, f],
-                    device_id={"fs": to},
-                    device_id_type=MESH,
-                )
-                pl.when(away)(copy.start)
-                pending.append((away, copy))
-
-                @pl.when(jnp.logical_not(away))
-                def _():
-                    full[kind, f] = held[b]
+            spread(kind, step).start()
+
+    @pl.when(z > 0)
+    def _():
+        pl.semaphore_wait(token, 1)
+
+    @pl.when(z < last)
+    def _():
+        pl.semaphore_signal(token, inc=1, device_id={"fs": f + 2}, device_id_type=MESH)
 
     def source(plane, i):
         r = (plane + 2 * shards - f) % planes
-        odd = (z + r) % 2
-        near = (i + 1) // 2
-        even_at = jnp.int32(2 * near if i % 2 else n_z - 2 * near)
-        odd_at = jnp.int32(1 + 2 * (i // 2) if i % 2 == 0 else n_z - 1 - 2 * (i // 2))
-        zs = (z + jnp.where(odd == 1, odd_at, even_at)) % n_z
+        zs = r % 2 + 2 * i
         return 2 * zs + ((zs + planes - r) // 2) % 2
+
+    def tell(i, carry):
+        at = source(x, i)
+
+        @pl.when(at // 2 < z)
+        def _():
+            pl.semaphore_signal(ready.at[f], inc=1, device_id={"fs": at}, device_id_type=MESH)
+
+        return carry
+
+    lax.fori_loop(0, sources, tell, 0)
+
+    s = first_block(x)
+
+    def along(kind, k):
+        to = planes * k + s
+        return to, pltpu.make_async_remote_copy(
+            src_ref=relay.at[kind, k // per_plane, k % per_plane],
+            dst_ref=full.at[kind, f],
+            send_sem=p2_send.at[kind, k],
+            recv_sem=full_recv.at[kind, f],
+            device_id={"fs": to},
+            device_id_type=MESH,
+        )
+
+    def send(kind, k):
+        a = k // per_plane
+        to, copy = along(kind, k)
+
+        @pl.when(jnp.logical_and(k % per_plane == 0, a != x))
+        def _():
+            pltpu.make_async_copy(src.at[kind, 0], relay.at[kind, a], p1_recv.at[kind, a]).wait()
+
+        if kind == 0:
+
+            @pl.when(to // 2 > z)
+            def _():
+                pl.semaphore_wait(ready.at[to], 1)
+
+        pl.when(to != f)(copy.start)
+
+        @pl.when(to == f)
+        def _():
+            full[kind, f] = relay[kind, a, k % per_plane]
 
     def arrived(kind, at):
         return pltpu.make_async_copy(full.at[kind, at], full.at[kind, at], full_recv.at[kind, at])
 
-    def forward(kind, at, step, sem):
-        copy = pltpu.make_async_remote_copy(
+    def hop(kind, at, step, sem):
+        return pltpu.make_async_remote_copy(
             src_ref=full.at[kind, at],
             dst_ref=full.at[kind, at],
             send_sem=sem,
@@ -180,24 +208,71 @@
             device_id={"tp": (x + step) % planes},
             device_id_type=MESH,
         )
-        copy.start()
-        pending.append((None, copy))
+
+    def forward(kind, i):
+        at = source(x, i)
+        pl.when(at != f)(arrived(kind, at).wait)
+        hop(kind, at, 1, p3_send.at[kind, i, 0]).start()
+        hop(kind, at, 3, p3_send.at[kind, i, 1]).start()
+
+    def pass_along(kind, i):
+        left = source((x + 3) % planes, i)
+        right = source((x + 1) % planes, i)
+        arrived(kind, left).wait()
+        pl.when(i % 2 == 0)(hop(kind, left, 1, p4_send.at[kind, i]).start)
+        arrived(kind, right).wait()
+        pl.when(i % 2 == 1)(hop(kind, right, 3, p4_send.at[kind, i]).start)
+
+    def loop(count, body):
+        def step(i, carry):
+            body(i)
+            return carry
+
+        lax.fori_loop(0, count, step, 0)
+
+    reach = z + ahead_by
+    for kind in range(2):
+
+        def near(j, kind=kind):
+            t = j // per_plane
+            a = (x + jnp.where(t == 1, 3, jnp.where(t == 0, 0, t - 1))) % planes
+            k = a * per_plane + j % per_plane
+            pl.when((planes * k + s) // 2 <= reach)(lambda: send(kind, k))
+
+        loop(sources, near)
+    for kind in range(2):
+
+        def near_forward(i, kind=kind):
+            pl.when(2 * i <= reach)(lambda: forward(kind, i))
+
+        def near_pass(i, kind=kind):
+            pl.when(2 * i <= reach)(lambda: pass_along(kind, i))
+
+        loop(sources, near_forward)
+        loop(sources, near_pass)
+
+    def far(k):
+        @pl.when(jnp.logical_and(k < sources, (planes * k + s) // 2 > reach))
+        def _():
+            send(0, k)
+            send(1, k)
+
+        @pl.when(jnp.logical_and(jnp.logical_and(k >= 1, k <= sources), 2 * (k - 1) > reach))
+        def _():
+            forward(0, k - 1)
+            forward(1, k - 1)
+
+        @pl.when(jnp.logical_and(k >= 2, 2 * (k - 2) > reach))
+        def _():
+            pass_along(0, k - 2)
+            pass_along(1, k - 2)
+
+    loop(sources + 2, far)
 
     def collect(kind):
-        for i in range(sources):
-            at = source(x, i)
-            pl.when(at != f)(arrived(kind, at).wait)
-            forward(kind, at, 1, p3_send.at[kind, i, 0])
-            forward(kind, at, 3, p3_send.at[kind, i, 1])
-        for i in range(sources):
-            for step, parity in ((3, 0), (1, 1)):
-                at = source((x + step) % planes, i)
-                arrived(kind, at).wait()
-                if i % 2 == parity:
-                    forward(kind, at, 4 - step, p4_send.at[kind, i])
-        for i in range(sources):
-            arrived(kind, source((x + 2) % planes, i)).wait()
-
+        loop(sources, lambda i: arrived(kind, source((x + 2) % planes, i)).wait())
+
+    pending = []
     collect(0)
     put_up = pltpu.make_async_copy(full.at[0], up_out, out_sem.at[0])
     put_up.start()
@@ -258,7 +333,7 @@
             device_id_type=MESH,
         )
         copy.start()
-        pending.append((None, copy))
+        pending.append(copy)
 
     pair[0].wait_recv()
     for slot in range(cut):
@@ -303,13 +378,23 @@
 
     put_up.wait()
     put_down.wait()
+    for kind in range(2):
+        for step in (1, 3, 2):
+            spread(kind, step).wait_send()
+
+        def drain(i, kind=kind):
+            to, copy = along(kind, i)
+            pl.when(to != f)(copy.wait_send)
+            at = source(x, i)
+            hop(kind, at, 1, p3_send.at[kind, i, 0]).wait_send()
+            hop(kind, at, 3, p3_send.at[kind, i, 1]).wait_send()
+            hop(kind, at, 1, p4_send.at[kind, i]).wait_send()
+
+        loop(sources, drain)
     for copy in pair:
         copy.wait_send()
-    for when, copy in pending:
-        if when is None:
-            copy.wait_send()
-        else:
-            pl.when(when)(copy.wait_send)
+    for copy in pending:
+        copy.wait_send()
 
 
 def local(shards, planes, tokens, norm_gain, up_trained, down_trained):
@@ -355,9 +440,11 @@
             dma((n_z,)),
             dma((n_z,)),
             dma((6,)),
+            pltpu.SemaphoreType.REGULAR,
+            pltpu.SemaphoreType.REGULAR((shards,)),
         ],
         compiler_params=pltpu.CompilerParams(
-            collective_id=0, has_side_effects=True, vmem_limit_bytes=48 * 1024 * 1024
+            collective_id=0, has_side_effects=True, vmem_limit_bytes=63 * 1024 * 1024
         ),
         name="handoff",
     )(tokens, norm_gain.reshape(1, rows), up_trained, down_trained)

time: 91.2 us -> 120 us (1.32)
  Pallas kernels: 83.3 us -> 114 us
  local copies, waits for them, and re-layouts: 6.51 us -> 4.82 us
    pallas_call x1, Pallas kernels: 83.3 us -> 114 us  [local(): pl.pallas_call(functools.partial(kernel, shards, planes), out_shape=(serv...]
    unnamed x11 -> x5, local copies, waits for them, and re-layouts: 6.51 us -> 4.82 us
where the time goes in v2:
time: 120 us; the launch traced here: 119 us
  Pallas kernels  114 us (95%)
  local copies, waits for them, and re-layouts  4.82 us (4%)
    pallas_call x1, Pallas kernels, local(): pl.pallas_call(functools.partial(kernel, shards, planes), out_shape=(serv...  114 us
    unnamed x5, local copies, waits for them, and re-layouts  4.82 us

profile of v2, /device:TPU:33, one launch (start us, length us, event | category | flops | bytes accessed | tf_op | source)
XLA Modules:
  0.0 119.3 jit_solution(1361202178078007331)
XLA Ops:
  0.6 113.9 %handoff.1 = (bf16[32,64,256]{2,1,0:T(8,128)(2,1)}, bf16[32,64,256]{2,1,0:T(8,128)(2,1)}, bf16[192,64]{1,0:T(8,128)(2,1)}) custom-call(bf16[192,2048]{1,0:T(8,128)(2,1)} %tok_hbm.1, f32[1,64]{1,0:T(1,128)} %bitcast.5, f32[64,2048]{1,0:T(8,128)} %up_hbm.1, f32[64,2048]{1,0:T(8,128)} %down_hbm.1), custom_call_target="tpu_custom_call" | custom-call | tf_op jit(solution)/shard_map/handoff/pallas_call | solution.py:411
  114.5 1.5 %copy.7 = bf16[192,64]{0,1:T(8,128)(2,1)} copy(bf16[192,64]{1,0:T(8,128)(2,1)} %get-tuple-element.11) | data formatting | bytes 49152
  116.0 0.0 copy-start
  116.0 2.4 %copy.10 = bf16[2048,256]{1,0:T(8,128)(2,1)} copy(bf16[2048,256]{1,0:T(8,128)(2,1)} %bitcast.4) | data formatting | bytes 2097152
  118.4 0.0 copy-done
  118.4 1.0 copy.11
Async XLA Ops:
  116.0 2.4 %copy-start = (bf16[32,64,256]{2,1,0:T(8,128)(2,1)S(1)}, bf16[32,64,256]{2,1,0:T(8,128)(2,1)}, u32[]{:S(2)}) copy-start(bf16[32,64,256]{2,1,0:T(8,128)(2,1)} %get-tuple-element.7) | copy-start | bytes 3145732

commit v3 on v1

v3 whole, which is shorter than its diff:
```python
import functools

import jax
import jax.numpy as jnp
from jax import lax
from jax.experimental import pallas as pl
from jax.experimental.pallas import tpu as pltpu
from jax.sharding import PartitionSpec as P

MESH = pl.DeviceIdType.MESH
epsilon = 1e-06


def ring_order(n):
    half = n // 2
    far = [d for d in range(half - 1, 3, -1)]
    slots, first = [half], {half: 0}
    for d in far + [2, 1, 3]:
        first[d] = len(slots)
        slots += [d, n - d]
    slots.append(0)
    return slots, first, 1 + 2 * len(far)


def kernel(
    shards,
    planes,
    tok_hbm,
    gain_hbm,
    up_hbm,
    down_hbm,
    up_out,
    down_out,
    y_ref,
    tok,
    gain,
    raw,
    normed,
    src,
    relay,
    full,
    mine,
    give,
    got,
    sums,
    stage,
    in_sem,
    out_sem,
    p1_send,
    p1_recv,
    p2_send,
    full_recv,
    p3_send,
    p4_send,
    pair_send,
    pair_recv,
    sum_send,
    stage_recv,
):
    f = lax.axis_index("fs")
    x = lax.axis_index("tp")
    n_z = shards // 2
    z = f // 2
    c = f % 2
    rows, width = full.shape[2], full.shape[3]

    def around(v, n):
        v = jnp.where(v >= n, v - n, v)
        return jnp.where(v < 0, v + n, v)

    per_plane = src.shape[2]
    blocks_here = planes * per_plane
    sources = shards // planes

    barrier = pltpu.get_barrier_semaphore()
    for step in range(1, planes):
        pl.semaphore_signal(barrier, inc=1, device_id={"tp": around(x + step, planes)}, device_id_type=MESH)

    def greet(step, carry):
        pl.semaphore_signal(barrier, inc=1, device_id={"fs": around(f + step, shards)}, device_id_type=MESH)
        return carry

    lax.fori_loop(1, shards, greet, 0)

    loads = [
        pltpu.make_async_copy(gain_hbm, gain, in_sem.at[0]),
        pltpu.make_async_copy(up_hbm, raw.at[0], in_sem.at[1]),
        pltpu.make_async_copy(down_hbm, raw.at[1], in_sem.at[2]),
        pltpu.make_async_copy(tok_hbm, tok, in_sem.at[3]),
    ]
    for load in loads:
        load.start()

    turn = (shards * planes - z - 2 * c) % planes

    def first_block(plane):
        return around(plane + turn, planes)

    loads[0].wait()
    row_at = lax.broadcasted_iota(jnp.int32, (rows, rows), 0)
    col_at = lax.broadcasted_iota(jnp.int32, (rows, rows), 1)
    column = jnp.sum(
        jnp.where(row_at == col_at, jnp.broadcast_to(gain[...], (rows, rows)), 0.0), axis=1, keepdims=True
    )

    def fold(kind):
        loads[1 + kind].wait()
        for step in (1, 3, 2, 0):
            plane = around(x + step, planes)
            for b in range(per_plane):
                at = pl.multiple_of((planes * b + first_block(plane)) * width, width)
                block = raw[kind, :, pl.ds(at, width)]
                if kind == 0:
                    block = block * column
                src[kind, plane, b] = block.astype(jnp.bfloat16)

    def norm():
        loads[3].wait()
        step_rows = 64
        for r in range(0, tok.shape[0], step_rows):
            values = tok[r : r + step_rows, :].astype(jnp.float32)
            scale = lax.rsqrt(jnp.mean(values * values, axis=1, keepdims=True) + epsilon)
            normed[r : r + step_rows, :] = (values * scale).astype(jnp.bfloat16)

    fold(0)
    fold(1)
    pl.semaphore_wait(barrier, planes - 1 + shards - 1)

    pending = []

    for kind in range(2):
        for step in (1, 3, 2):
            plane = around(x + step, planes)
            copy = pltpu.make_async_remote_copy(
                src_ref=src.at[kind, plane],
                dst_ref=relay.at[kind, x],
                send_sem=p1_send.at[kind, step - 1],
                recv_sem=p1_recv.at[kind, x],
                device_id={"tp": plane},
                device_id_type=MESH,
            )
            copy.start()
            pending.append((None, copy))

    s = first_block(x)
    lift = s // 2

    def taken(kind, a):
        pltpu.make_async_copy(src.at[kind, 0], relay.at[kind, a], p1_recv.at[kind, a]).wait()

    def along(kind, k, held, n):
        to = planes * k + s
        away = to != f
        copy = pltpu.make_async_remote_copy(
            src_ref=held,
            dst_ref=full.at[kind, f],
            send_sem=p2_send.at[kind, n],
            recv_sem=full_recv.at[kind, f],
            device_id={"fs": to},
            device_id_type=MESH,
        )
        pl.when(away)(copy.start)
        pending.append((away, copy))

        @pl.when(jnp.logical_not(away))
        def _():
            full[kind, f] = held[...]

    for step in (0, 3, 1, 2):
        a = around(x + step, planes)
        if step > 0:
            taken(0, a)
        for b in range(per_plane):
            held = src.at[0, x, b] if step == 0 else relay.at[0, a, b]
            along(0, per_plane * a + b, held, step * per_plane + b)

    relay[1, x] = src[1, x]
    norm()

    hops = [2 * ((i + 1) // 2) if i % 2 == 0 else -2 * ((i + 1) // 2) for i in range(sources)]

    def sources_of(plane):
        r = (plane + 2 * shards - f) % planes
        odd = (z + r) % 2
        base = ((z + odd + planes - r) // 2) % 2
        found = []
        for ahead in hops:
            core = base if (ahead // 2) % 2 == 0 else 1 - base
            found.append(2 * around(z + odd + ahead, n_z) + core)
        return found

    own, right, across, left = [sources_of(around(x + step, planes)) for step in range(planes)]
    beyond = list(range(sources - 1, -1, -1))

    def arrived(kind, at):
        return pltpu.make_async_copy(full.at[kind, at], full.at[kind, at], full_recv.at[kind, at])

    def forward(kind, at, step, sem):
        copy = pltpu.make_async_remote_copy(
            src_ref=full.at[kind, at],
            dst_ref=full.at[kind, at],
            send_sem=sem,
            recv_sem=full_recv.at[kind, at],
            device_id={"tp": around(x + step, planes)},
            device_id_type=MESH,
        )
        copy.start()
        pending.append((None, copy))

    def to_sides(kind, some):
        for i in some:
            at = own[i]
            pl.when(at != f)(arrived(kind, at).wait)
            forward(kind, at, 1, p3_send.at[kind, i, 0])
            forward(kind, at, 3, p3_send.at[kind, i, 1])

    def from_sides(kind, some):
        for i in some:
            for found, step, parity in ((left, 1, 0), (right, 3, 1)):
                at = found[i]
                arrived(kind, at).wait()
                if i % 2 == parity:
                    forward(kind, at, step, p4_send.at[kind, i])

    def from_across(kind, some):
        for i in some:
            arrived(kind, across[i]).wait()

    near_at = jnp.where(z < lift, lift - z, z - lift) % 2
    near = z + near_at
    for a in range(planes):
        pl.when(a != x)(functools.partial(taken, 1, a))
    for n, i in enumerate(beyond):
        k = (around(near + hops[i], n_z) - lift) // 2
        along(1, k, relay.at[1, k // per_plane, k % per_plane], n)

    everything = list(range(sources))
    to_sides(0, everything)
    from_sides(0, everything)
    from_across(0, everything)
    put_up = pltpu.make_async_copy(full.at[0], up_out, out_sem.at[0])
    put_up.start()
    up = full[0].reshape(shards * rows, width)
    hidden = jnp.dot(normed[...], up, preferred_element_type=jnp.float32)
    active = jnp.square(jnp.maximum(hidden, 0.0)).astype(jnp.bfloat16)

    half = tok.shape[0] // 2
    low = lax.broadcasted_iota(jnp.int32, (half, 2 * rows), 1) < rows
    slots, first, cut = ring_order(n_z)

    def part_of(slot):
        owner = around(z + slots[slot], n_z)
        block = full[1, pl.ds(2 * owner, 2)].reshape(2 * rows, width)
        part = lax.dot_general(active, block, (((1,), (1,)), ((), ())), preferred_element_type=jnp.float32)
        top, bottom = part[:half], part[half:]
        even = jnp.where(low, top, pltpu.roll(bottom, rows, 1))
        odd = jnp.where(low, pltpu.roll(top, rows, 1), bottom)
        mine[slot] = jnp.where(c == 0, even, odd)
        give[slot] = jnp.where(c == 0, odd, even).astype(jnp.bfloat16)

    def exchange(j, start, stop):
        copy = pltpu.make_async_remote_copy(
            src_ref=give.at[pl.ds(start, stop - start)],
            dst_ref=got.at[pl.ds(start, stop - start)],
            send_sem=pair_send.at[j],
            recv_sem=pair_recv.at[j],
            device_id={"fs": f + 1 - 2 * c},
            device_id_type=MESH,
        )
        copy.start()
        pending.append((None, copy))
        return copy

    top_d = n_z // 2
    sign = 1 - 2 * c

    def place(side, d):
        if d == top_d:
            return 0
        return first[d] + (c if side == 0 else 1 - c)

    count = [0]
    stage_at = {}

    def pass_on(side, d, target):
        j = count[0]
        count[0] += 1
        stage_at[(side, d)] = j
        to = around(z + (sign if side == 0 else -sign) * (d - target), n_z)
        copy = pltpu.make_async_remote_copy(
            src_ref=sums.at[place(side, d)],
            dst_ref=stage.at[j],
            send_sem=sum_send.at[j],
            recv_sem=stage_recv.at[j],
            device_id={"fs": 2 * to + c},
            device_id_type=MESH,
        )
        copy.start()
        pending.append((None, copy))

    def add_up(side, d, below):
        slot = place(side, d)
        total = mine[slot] + got[slot].astype(jnp.float32)
        for e in below:
            j = stage_at[(side, e)]
            pltpu.make_async_copy(stage.at[j], stage.at[j], stage_recv.at[j]).wait()
            total = total + stage[j].astype(jnp.float32)
        return total

    def settle(side, d, below=()):
        sums[place(side, d)] = add_up(side, d, below).astype(jnp.bfloat16)

    far = beyond[:5]
    close = beyond[5:]
    to_sides(1, far)
    from_sides(1, far)
    from_across(1, far)
    for slot in range(cut):
        part_of(slot)
    pair_far = exchange(0, 0, cut)
    to_sides(1, close)
    pair_far.wait_recv()
    leaves = [(0, top_d, 6), (0, 7, 6), (1, 7, 6), (0, 5, 4), (1, 5, 4)]
    for side, d, target in leaves:
        settle(side, d)
    for side, d, target in leaves:
        pass_on(side, d, target)
    from_sides(1, close)
    from_across(1, close)
    put_down = pltpu.make_async_copy(full.at[1], down_out, out_sem.at[1])
    put_down.start()
    settle(0, 6, (top_d, 7))
    settle(1, 6, (7,))
    pass_on(0, 6, 3)
    pass_on(1, 6, 3)
    settle(0, 4, (5,))
    settle(1, 4, (5,))
    pass_on(0, 4, 3)
    pass_on(1, 4, 3)
    for slot in range(cut, n_z):
        part_of(slot)
    pair_near = exchange(1, cut, n_z)
    pair_near.wait_recv()
    for d in (2, 1):
        for side in range(2):
            settle(side, d)
    for d in (2, 1):
        for side in range(2):
            pass_on(side, d, 0)
    for side in range(2):
        settle(side, 3, (6, 4))
        pass_on(side, 3, 0)
    home = n_z - 1
    total = mine[home] + got[home].astype(jnp.float32)
    for d in (1, 2, 3):
        for side in range(2):
            j = stage_at[(side, d)]
            pltpu.make_async_copy(stage.at[j], stage.at[j], stage_recv.at[j]).wait()
            total = total + stage[j].astype(jnp.float32)
    total = total.T
    y_ref[:, 0:half] = total[0:rows].astype(jnp.bfloat16)
    y_ref[:, half : 2 * half] = total[rows : 2 * rows].astype(jnp.bfloat16)

    put_up.wait()
    put_down.wait()
    for when, copy in pending:
        if when is None:
            copy.wait_send()
        else:
            pl.when(when)(copy.wait_send)


def local(shards, planes, tokens, norm_gain, up_trained, down_trained):
    rows, cols = up_trained.shape
    count, depth = tokens.shape
    width = cols * planes // shards
    per_plane = cols // width // planes
    n_z = shards // 2
    half = count // 2
    bf16, f32 = jnp.bfloat16, jnp.float32
    served = jax.ShapeDtypeStruct((shards, rows, width), bf16)
    dma = pltpu.SemaphoreType.DMA
    any_space = pl.BlockSpec(memory_space=pl.ANY)
    up, down, y = pl.pallas_call(
        functools.partial(kernel, shards, planes),
        out_shape=(served, served, jax.ShapeDtypeStruct((rows, count), bf16)),
        in_specs=[any_space] * 4,
        out_specs=(any_space, any_space, pl.BlockSpec(memory_space=pltpu.VMEM)),
        scratch_shapes=[
            pltpu.VMEM((count, depth), bf16),
            pltpu.VMEM((1, rows), f32),
            pltpu.VMEM((2, rows, cols), f32),
            pltpu.VMEM((count, depth), bf16),
            pltpu.VMEM((2, planes, per_plane, rows, width), bf16),
            pltpu.VMEM((2, planes, per_plane, rows, width), bf16),
            pltpu.VMEM((2, shards, rows, width), bf16),
            pltpu.VMEM((n_z, half, 2 * rows), f32),
            pltpu.VMEM((n_z, half, 2 * rows), bf16),
            pltpu.VMEM((n_z, half, 2 * rows), bf16),
            pltpu.VMEM((n_z, half, 2 * rows), bf16),
            pltpu.VMEM((n_z, half, 2 * rows), bf16),
            dma((4,)),
            dma((2,)),
            dma((2, planes - 1)),
            dma((2, planes)),
            dma((2, planes * per_plane)),
            dma((2, shards)),
            dma((2, shards // planes, 2)),
            dma((2, shards // planes)),
            dma((2,)),
            dma((2,)),
            dma((n_z,)),
            dma((n_z,)),
        ],
        compiler_params=pltpu.CompilerParams(
            collective_id=0, has_side_effects=True, vmem_limit_bytes=63 * 1024 * 1024
        ),
        name="handoff",
    )(tokens, norm_gain.reshape(1, rows), up_trained, down_trained)
    return (up.reshape(shards * rows, width), down.reshape(shards * rows, width), y.T)


def solution(mesh):
    in_specs = (P(("grp", "tp"), None), P("fs"), P("fs", "tp"), P("fs", "tp"))
    out_specs = (P("grp", "fs"), P("grp", "fs"), P(("grp", "tp"), "fs"))
    body = functools.partial(local, mesh.shape["fs"], mesh.shape["tp"])
    return jax.shard_map(body, mesh=mesh, in_specs=in_specs, out_specs=out_specs, check_vma=False)
```

time: 91.2 us -> 95.5 us (1.047)
  Pallas kernels: 83.3 us -> 90.7 us
  local copies, waits for them, and re-layouts: 6.51 us -> 3.94 us
    pallas_call x1, Pallas kernels: 83.3 us -> 90.7 us  [local(): pl.pallas_call(functools.partial(kernel, shards, planes), out_shape=(serv...]
    unnamed x11 -> x7, local copies, waits for them, and re-layouts: 6.51 us -> 3.94 us
where the time goes in v3:
time: 95.5 us; the launch traced here: 95.3 us
  Pallas kernels  90.7 us (95%)
  local copies, waits for them, and re-layouts  3.94 us (4%)
    pallas_call x1, Pallas kernels, local(): pl.pallas_call(functools.partial(kernel, shards, planes), out_shape=(serv...  90.7 us
    unnamed x7, local copies, waits for them, and re-layouts  3.94 us

profile of v3, /device:TPU:33, one launch (start us, length us, event | category | flops | bytes accessed | tf_op | source)
XLA Modules:
  0.0 95.3 jit_solution(13178974390579486463)
XLA Ops:
  0.6 90.7 %handoff.1 = (bf16[32,64,256]{2,1,0:T(8,128)(2,1)}, bf16[32,64,256]{2,1,0:T(8,128)(2,1)}, bf16[64,192]{1,0:T(8,128)(2,1)}) custom-call(bf16[192,2048]{1,0:T(8,128)(2,1)} %tok_hbm.1, f32[1,64]{1,0:T(1,128)} %bitcast.7, f32[64,2048]{1,0:T(8,128)} %up_hbm.1, f32[64,2048]{1,0:T(8,128)} %down_hbm.1), custom_call_target="tpu_custom_call" | custom-call | tf_op jit(solution)/shard_map/handoff/pallas_call | solution.py:384
  91.4 0.0 copy-start
  91.4 2.4 %copy.10 = bf16[2048,256]{1,0:T(8,128)(2,1)} copy(bf16[2048,256]{1,0:T(8,128)(2,1)} %bitcast.5) | data formatting | bytes 2097152
  93.7 0.0 copy-done
  93.7 0.0 copy-start.1
  93.7 1.0 %copy.11 = bf16[2048,256]{1,0:T(8,128)(2,1)} copy(bf16[2048,256]{1,0:T(8,128)(2,1)S(1)} %bitcast.4) | data formatting | bytes 2097152
  94.7 0.0 copy-done.1
  94.7 0.6 copy.12
Async XLA Ops:
  91.4 2.4 %copy-start = (bf16[32,64,256]{2,1,0:T(8,128)(2,1)S(1)}, bf16[32,64,256]{2,1,0:T(8,128)(2,1)}, u32[]{:S(2)}) copy-start(bf16[32,64,256]{2,1,0:T(8,128)(2,1)} %get-tuple-element.7) | copy-start | bytes 3145732
  93.7 1.0 %copy-start.1 = (bf16[64,192]{1,0:T(8,128)(2,1)S(1)}, bf16[64,192]{1,0:T(8,128)(2,1)}, u32[]{:S(2)}) copy-start(bf16[64,192]{1,0:T(8,128)(2,1)} %get-tuple-element.8) | copy-start | bytes 73732

commit v4 on v3

--- a/solution.py
+++ b/solution.py
@@ -9,6 +9,7 @@
 
 MESH = pl.DeviceIdType.MESH
 epsilon = 1e-06
+behind = 5.0
 
 
 def ring_order(n):
@@ -38,14 +39,12 @@
     normed,
     src,
     relay,
-    full,
     mine,
     give,
     got,
     sums,
     stage,
     in_sem,
-    out_sem,
     p1_send,
     p1_recv,
     p2_send,
@@ -56,13 +55,24 @@
     pair_recv,
     sum_send,
     stage_recv,
+    token,
+    ready,
+    active,
 ):
     f = lax.axis_index("fs")
     x = lax.axis_index("tp")
     n_z = shards // 2
     z = f // 2
     c = f % 2
-    rows, width = full.shape[2], full.shape[3]
+    rows, width = up_out.shape[1], up_out.shape[2]
+
+    full = (up_out, down_out)
+
+    def when(flag):
+        return (lambda body: body()) if flag is True else pl.when(flag)
+
+    def both(a, b):
+        return b if a is True else jnp.logical_and(a, b)
 
     def around(v, n):
         v = jnp.where(v >= n, v - n, v)
@@ -72,15 +82,15 @@
     blocks_here = planes * per_plane
     sources = shards // planes
 
+    last = n_z - 1
     barrier = pltpu.get_barrier_semaphore()
     for step in range(1, planes):
         pl.semaphore_signal(barrier, inc=1, device_id={"tp": around(x + step, planes)}, device_id_type=MESH)
-
-    def greet(step, carry):
-        pl.semaphore_signal(barrier, inc=1, device_id={"fs": around(f + step, shards)}, device_id_type=MESH)
-        return carry
-
-    lax.fori_loop(1, shards, greet, 0)
+    pl.semaphore_signal(barrier, inc=1, device_id={"fs": f + 1 - 2 * c}, device_id_type=MESH)
+
+    @pl.when(z == 0)
+    def _():
+        pl.semaphore_signal(barrier, inc=1, device_id={"fs": f + 2 * last}, device_id_type=MESH)
 
     loads = [
         pltpu.make_async_copy(gain_hbm, gain, in_sem.at[0]),
@@ -122,65 +132,43 @@
             scale = lax.rsqrt(jnp.mean(values * values, axis=1, keepdims=True) + epsilon)
             normed[r : r + step_rows, :] = (values * scale).astype(jnp.bfloat16)
 
-    fold(0)
-    fold(1)
-    pl.semaphore_wait(barrier, planes - 1 + shards - 1)
+    pl.semaphore_wait(barrier, planes + jnp.where(z > 1, 1, 0) + jnp.where(z == last, 1, 0))
+
+    @pl.when(jnp.logical_and(z > 0, z < last))
+    def _():
+        pl.semaphore_signal(barrier, inc=1, device_id={"fs": f + 2}, device_id_type=MESH)
+
+    @pl.when(z == last)
+    def _():
+        pl.semaphore_signal(token, inc=1, device_id={"fs": f - 2 * last}, device_id_type=MESH)
+
 
     pending = []
 
-    for kind in range(2):
-        for step in (1, 3, 2):
-            plane = around(x + step, planes)
-            copy = pltpu.make_async_remote_copy(
-                src_ref=src.at[kind, plane],
-                dst_ref=relay.at[kind, x],
-                send_sem=p1_send.at[kind, step - 1],
-                recv_sem=p1_recv.at[kind, x],
-                device_id={"tp": plane},
-                device_id_type=MESH,
-            )
-            copy.start()
-            pending.append((None, copy))
-
-    s = first_block(x)
-    lift = s // 2
-
-    def taken(kind, a):
-        pltpu.make_async_copy(src.at[kind, 0], relay.at[kind, a], p1_recv.at[kind, a]).wait()
-
-    def along(kind, k, held, n):
-        to = planes * k + s
-        away = to != f
-        copy = pltpu.make_async_remote_copy(
-            src_ref=held,
-            dst_ref=full.at[kind, f],
-            send_sem=p2_send.at[kind, n],
-            recv_sem=full_recv.at[kind, f],
-            device_id={"fs": to},
-            device_id_type=MESH,
-        )
-        pl.when(away)(copy.start)
-        pending.append((away, copy))
-
-        @pl.when(jnp.logical_not(away))
-        def _():
-            full[kind, f] = held[...]
-
-    for step in (0, 3, 1, 2):
-        a = around(x + step, planes)
-        if step > 0:
-            taken(0, a)
+    def spread(kind):
+        fold(kind)
         for b in range(per_plane):
-            held = src.at[0, x, b] if step == 0 else relay.at[0, a, b]
-            along(0, per_plane * a + b, held, step * per_plane + b)
-
-    relay[1, x] = src[1, x]
-    norm()
+            for step in (1, 3, 2):
+                plane = around(x + step, planes)
+                copy = pltpu.make_async_remote_copy(
+                    src_ref=src.at[kind, plane, b],
+                    dst_ref=relay.at[kind, x, b],
+                    send_sem=p1_send.at[kind, step - 1, b],
+                    recv_sem=p1_recv.at[kind, x, b],
+                    device_id={"tp": plane},
+                    device_id_type=MESH,
+                )
+                copy.start()
+                pending.append((None, copy))
+        relay[kind, x] = src[kind, x]
 
     hops = [2 * ((i + 1) // 2) if i % 2 == 0 else -2 * ((i + 1) // 2) for i in range(sources)]
 
+    def turn_of(plane):
+        return (plane + 2 * shards - f) % planes
+
     def sources_of(plane):
-        r = (plane + 2 * shards - f) % planes
+        r = turn_of(plane)
         odd = (z + r) % 2
         base = ((z + odd + planes - r) // 2) % 2
         found = []
@@ -191,58 +179,121 @@
 
     own, right, across, left = [sources_of(around(x + step, planes)) for step in range(planes)]
     beyond = list(range(sources - 1, -1, -1))
+    def tell():
+        for at in own:
+
+            @pl.when(jnp.logical_and(at >= 2, jnp.logical_or(at < 2 * z, z == 0)))
+            def _():
+                pl.semaphore_signal(ready.at[f], inc=1, device_id={"fs": at}, device_id_type=MESH)
+
+    pl.when(z > 0)(tell)
+    spread(0)
+    spread(1)
+
+    @pl.when(z == 0)
+    def _():
+        pl.semaphore_wait(token, 1)
+        tell()
+
+    s = first_block(x)
+    lift = s // 2
+
+    def taken(kind, a, b):
+        here = relay.at[kind, a, b]
+        pltpu.make_async_copy(here, here, p1_recv.at[kind, a, b]).wait()
+
+    def along(kind, a, b, n, wanted=True):
+        to = blocks_here * a + planes * b + s
+        away = both(wanted, to != f)
+        held = relay.at[kind, a, b]
+        copy = pltpu.make_async_remote_copy(
+            src_ref=held,
+            dst_ref=full[kind].at[f],
+            send_sem=p2_send.at[kind, n],
+            recv_sem=full_recv.at[kind, f],
+            device_id={"fs": to},
+            device_id_type=MESH,
+        )
+        pl.when(both(wanted, a != x))(lambda: taken(kind, a, b))
+        if kind == 0:
+
+            @pl.when(both(wanted, jnp.logical_and(z > 0, jnp.logical_or(to > 2 * z + 1, to < 2))))
+            def _():
+                pl.semaphore_wait(ready.at[to], 1)
+
+        pl.when(away)(copy.start)
+        pending.append((away, copy))
+
+        @pl.when(both(wanted, to == f))
+        def _():
+            full[kind][f] = held[...]
+
+    norm()
 
     def arrived(kind, at):
-        return pltpu.make_async_copy(full.at[kind, at], full.at[kind, at], full_recv.at[kind, at])
+        return pltpu.make_async_copy(full[kind].at[at], full[kind].at[at], full_recv.at[kind, at])
 
     def forward(kind, at, step, sem):
         copy = pltpu.make_async_remote_copy(
-            src_ref=full.at[kind, at],
-            dst_ref=full.at[kind, at],
+            src_ref=full[kind].at[at],
+            dst_ref=full[kind].at[at],
             send_sem=sem,
             recv_sem=full_recv.at[kind, at],
             device_id={"tp": around(x + step, planes)},
             device_id_type=MESH,
         )
-        copy.start()
-        pending.append((None, copy))
-
-    def to_sides(kind, some):
-        for i in some:
-            at = own[i]
-            pl.when(at != f)(arrived(kind, at).wait)
-            forward(kind, at, 1, p3_send.at[kind, i, 0])
-            forward(kind, at, 3, p3_send.at[kind, i, 1])
-
-    def from_sides(kind, some):
-        for i in some:
-            for found, step, parity in ((left, 1, 0), (right, 3, 1)):
-                at = found[i]
+        return copy
+
+    early = n_z - n_z // 4
+    late = list(range(sources, sources + sources // 4))
+
+    def of_slot(step, i):
+        if i < sources:
+            at = (own, right, across, left)[step][i]
+            return at, jnp.logical_and(at >= 2, at < 2 * early + 2)
+        r = turn_of(around(x + step, planes))
+        zs = around(early + 1 + 2 * (i - sources) + (r + early + 1) % 2, n_z)
+        return 2 * zs + ((zs + planes - r) // 2) % 2, True
+
+    def to_sides(kind, i):
+        at, stands = of_slot(0, i)
+
+        @when(stands)
+        def _():
+            pl.when(at != f)(lambda: arrived(kind, at).wait())
+            forward(kind, at, 1, p3_send.at[kind, i, 0]).start()
+            forward(kind, at, 3, p3_send.at[kind, i, 1]).start()
+
+        pending.append((stands, forward(kind, at, 1, p3_send.at[kind, i, 0])))
+        pending.append((stands, forward(kind, at, 3, p3_send.at[kind, i, 1])))
+
+    def from_sides(kind, i):
+        for from_step, to_step, parity in ((3, 1, 0), (1, 3, 1)):
+            at, stands = of_slot(from_step, i)
+            turned = (at // 4) % 2 == parity
+            sem = p4_send.at[kind, i, parity]
+
+            @when(stands)
+            def _():
                 arrived(kind, at).wait()
-                if i % 2 == parity:
-                    forward(kind, at, step, p4_send.at[kind, i])
+                pl.when(turned)(lambda: forward(kind, at, to_step, sem).start())
+
+            pending.append((both(stands, turned), forward(kind, at, to_step, sem)))
 
     def from_across(kind, some):
         for i in some:
-            arrived(kind, across[i]).wait()
-
-    near_at = jnp.where(z < lift, lift - z, z - lift) % 2
-    near = z + near_at
-    for a in range(planes):
-        pl.when(a != x)(functools.partial(taken, 1, a))
-    for n, i in enumerate(beyond):
-        k = (around(near + hops[i], n_z) - lift) // 2
-        along(1, k, relay.at[1, k // per_plane, k % per_plane], n)
-
+            at, stands = of_slot(2, i)
+            when(stands)(lambda: arrived(kind, at).wait())
+
+    near = z + jnp.where(z < lift, lift - z, z - lift) % 2
     everything = list(range(sources))
-    to_sides(0, everything)
-    from_sides(0, everything)
-    from_across(0, everything)
-    put_up = pltpu.make_async_copy(full.at[0], up_out, out_sem.at[0])
-    put_up.start()
-    up = full[0].reshape(shards * rows, width)
-    hidden = jnp.dot(normed[...], up, preferred_element_type=jnp.float32)
-    active = jnp.square(jnp.maximum(hidden, 0.0)).astype(jnp.bfloat16)
+    for b in range(per_plane):
+        along(0, x, b, sources + b)
+    for kind, some in ((0, everything), (1, beyond)):
+        for i in some:
+            k = (around(near + hops[i], n_z) - lift) // 2
+            a = k // per_plane
+            along(kind, a, k % per_plane, i, a != x if kind == 0 else True)
 
     half = tok.shape[0] // 2
     low = lax.broadcasted_iota(jnp.int32, (half, 2 * rows), 1) < rows
@@ -250,8 +301,8 @@
 
     def part_of(slot):
         owner = around(z + slots[slot], n_z)
-        block = full[1, pl.ds(2 * owner, 2)].reshape(2 * rows, width)
-        part = lax.dot_general(active, block, (((1,), (1,)), ((), ())), preferred_element_type=jnp.float32)
+        block = down_out[pl.ds(2 * owner, 2)].reshape(2 * rows, width)
+        part = lax.dot_general(active[...], block, (((1,), (1,)), ((), ())), preferred_element_type=jnp.float32)
         top, bottom = part[:half], part[half:]
         even = jnp.where(low, top, pltpu.roll(bottom, rows, 1))
         odd = jnp.where(low, pltpu.roll(top, rows, 1), bottom)
@@ -310,25 +361,45 @@
     def settle(side, d, below=()):
         sums[place(side, d)] = add_up(side, d, below).astype(jnp.bfloat16)
 
-    far = beyond[:5]
+    far = beyond[:5] + late
     close = beyond[5:]
-    to_sides(1, far)
-    from_sides(1, far)
-    from_across(1, far)
-    for slot in range(cut):
-        part_of(slot)
-    pair_far = exchange(0, 0, cut)
-    to_sides(1, close)
-    pair_far.wait_recv()
+    pair = []
+
+    def finish_up():
+        from_across(0, everything + late)
+        up = up_out[...].reshape(shards * rows, width)
+        hidden = jnp.dot(normed[...], up, preferred_element_type=jnp.float32)
+        active[...] = jnp.square(jnp.maximum(hidden, 0.0)).astype(jnp.bfloat16)
+
+    def far_sums():
+        from_across(1, far)
+        for slot in range(cut):
+            part_of(slot)
+        pair.append(exchange(0, 0, cut))
+
+    events = []
+    for n in range(sources):
+        events.append((6.5 + 1.6 * n, to_sides, 0, n))
+        events.append((6.5 + behind + 1.6 * n, from_sides, 0, n))
+    for n, i in enumerate(late):
+        events.append((16.0 + n, to_sides, 0, i))
+        events.append((16.0 + behind + n, from_sides, 0, i))
+        events.append((24.4 + 0.5 * n, to_sides, 1, i))
+        events.append((24.4 + behind + 0.1 * n, from_sides, 1, i))
+    for n, i in enumerate(beyond):
+        events.append((19.0 + 1.2 * n, to_sides, 1, i))
+        events.append((19.0 + behind + 1.2 * n, from_sides, 1, i))
+    events.append((24.95 + behind, lambda *_: finish_up(), 0, 0))
+    events.append((26.2 + behind, lambda *_: far_sums(), 0, 0))
+    for _, act, kind, i in sorted(events, key=lambda event: event[0]):
+        act(kind, i)
+    pair[0].wait_recv()
     leaves = [(0, top_d, 6), (0, 7, 6), (1, 7, 6), (0, 5, 4), (1, 5, 4)]
     for side, d, target in leaves:
         settle(side, d)
     for side, d, target in leaves:
         pass_on(side, d, target)
-    from_sides(1, close)
     from_across(1, close)
-    put_down = pltpu.make_async_copy(full.at[1], down_out, out_sem.at[1])
-    put_down.start()
     settle(0, 6, (top_d, 7))
     settle(1, 6, (7,))
     pass_on(0, 6, 3)
@@ -361,10 +432,8 @@
     y_ref[:, 0:half] = total[0:rows].astype(jnp.bfloat16)
     y_ref[:, half : 2 * half] = total[rows : 2 * rows].astype(jnp.bfloat16)
 
-    put_up.wait()
-    put_down.wait()
     for when, copy in pending:
-        if when is None:
+        if when is None or when is True:
             copy.wait_send()
         else:
             pl.when(when)(copy.wait_send)
@@ -378,14 +447,14 @@
     n_z = shards // 2
     half = count // 2
     bf16, f32 = jnp.bfloat16, jnp.float32
-    served = jax.ShapeDtypeStruct((shards, rows, width), bf16)
+    served = pltpu.VMEM((shards, rows, width), bf16)
     dma = pltpu.SemaphoreType.DMA
     any_space = pl.BlockSpec(memory_space=pl.ANY)
     up, down, y = pl.pallas_call(
         functools.partial(kernel, shards, planes),
         out_shape=(served, served, jax.ShapeDtypeStruct((rows, count), bf16)),
         in_specs=[any_space] * 4,
-        out_specs=(any_space, any_space, pl.BlockSpec(memory_space=pltpu.VMEM)),
+        out_specs=(pl.BlockSpec(memory_space=pltpu.VMEM),) * 3,
         scratch_shapes=[
             pltpu.VMEM((count, depth), bf16),
             pltpu.VMEM((1, rows), f32),
@@ -393,27 +462,28 @@
             pltpu.VMEM((count, depth), bf16),
             pltpu.VMEM((2, planes, per_plane, rows, width), bf16),
             pltpu.VMEM((2, planes, per_plane, rows, width), bf16),
-            pltpu.VMEM((2, shards, rows, width), bf16),
             pltpu.VMEM((n_z, half, 2 * rows), f32),
             pltpu.VMEM((n_z, half, 2 * rows), bf16),
             pltpu.VMEM((n_z, half, 2 * rows), bf16),
             pltpu.VMEM((n_z, half, 2 * rows), bf16),
             pltpu.VMEM((n_z, half, 2 * rows), bf16),
             dma((4,)),
-            dma((2,)),
-            dma((2, planes - 1)),
-            dma((2, planes)),
-            dma((2, planes * per_plane)),
+            dma((2, planes - 1, per_plane)),
+            dma((2, planes, per_plane)),
+            dma((2, planes * per_plane + per_plane)),
             dma((2, shards)),
-            dma((2, shards // planes, 2)),
-            dma((2, shards // planes)),
+            dma((2, shards // planes * 5 // 4, 2)),
+            dma((2, shards // planes * 5 // 4, 2)),
             dma((2,)),
             dma((2,)),
             dma((n_z,)),
             dma((n_z,)),
+            pltpu.SemaphoreType.REGULAR,
+            pltpu.SemaphoreType.REGULAR((shards,)),
+            pltpu.VMEM((count, width), bf16),
         ],
         compiler_params=pltpu.CompilerParams(
-            collective_id=0, has_side_effects=True, vmem_limit_bytes=63 * 1024 * 1024
+            collective_id=0, has_side_effects=True, vmem_limit_bytes=61 * 1024 * 1024
         ),
         name="handoff",
     )(tokens, norm_gain.reshape(1, rows), up_trained, down_trained)

time: 95.5 us -> 86.5 us (0.906)
  Pallas kernels: 90.7 us -> 83.1 us
  local copies, waits for them, and re-layouts: 3.94 us -> 2.56 us
    pallas_call x1, Pallas kernels: 90.7 us -> 83.1 us  [local(): pl.pallas_call(functools.partial(kernel, shards, planes), out_shape=(serv...]
    unnamed x7 -> x5, local copies, waits for them, and re-layouts: 3.94 us -> 2.56 us
where the time goes in v4:
time: 86.5 us; the launch traced here: 86.3 us
  Pallas kernels  83.1 us (96%)
  local copies, waits for them, and re-layouts  2.56 us (3%)
    pallas_call x1, Pallas kernels, local(): pl.pallas_call(functools.partial(kernel, shards, planes), out_shape=(serv...  83.1 us
    unnamed x5, local copies, waits for them, and re-layouts  2.56 us

profile of v4, /device:TPU:33, one launch (start us, length us, event | category | flops | bytes accessed | tf_op | source)
XLA Modules:
  0.0 86.3 jit_solution(539090129940521591)
XLA Ops:
  0.6 83.1 %handoff.1 = (bf16[32,64,256]{2,1,0:T(8,128)(2,1)S(1)}, bf16[32,64,256]{2,1,0:T(8,128)(2,1)S(1)}, bf16[64,192]{1,0:T(8,128)(2,1)}) custom-call(bf16[192,2048]{1,0:T(8,128)(2,1)} %tok_hbm.1, f32[1,64]{1,0:T(1,128)} %bitcast.7, f32[64,2048]{1,0:T(8,128)} %up_hbm.1, f32[64,2048]{1,0:T(8,128)} %down_hbm.1), custom_call_target="tpu_custom_call" | custom-call | tf_op jit(solution)/shard_map/handoff/pallas_call | solution.py:453
  83.8 1.0 %copy.10 = bf16[2048,256]{1,0:T(8,128)(2,1)} copy(bf16[2048,256]{1,0:T(8,128)(2,1)S(1)} %bitcast.5) | data formatting | bytes 2097152
  84.7 0.0 copy-start
  84.7 1.0 %copy.11 = bf16[2048,256]{1,0:T(8,128)(2,1)} copy(bf16[2048,256]{1,0:T(8,128)(2,1)S(1)} %bitcast.4) | data formatting | bytes 2097152
  85.7 0.0 copy-done
  85.7 0.6 copy.12
Async XLA Ops:
  84.7 1.0 %copy-start = (bf16[64,192]{1,0:T(8,128)(2,1)S(1)}, bf16[64,192]{1,0:T(8,128)(2,1)}, u32[]{:S(2)}) copy-start(bf16[64,192]{1,0:T(8,128)(2,1)} %get-tuple-element.8) | copy-start | bytes 73732

commit v5 on v4

--- a/solution.py
+++ b/solution.py
@@ -88,9 +88,15 @@
         pl.semaphore_signal(barrier, inc=1, device_id={"tp": around(x + step, planes)}, device_id_type=MESH)
     pl.semaphore_signal(barrier, inc=1, device_id={"fs": f + 1 - 2 * c}, device_id_type=MESH)
 
-    @pl.when(z == 0)
-    def _():
-        pl.semaphore_signal(barrier, inc=1, device_id={"fs": f + 2 * last}, device_id_type=MESH)
+    def greet(at, carry):
+        @pl.when(jnp.logical_or(jnp.logical_and(z > 0, at > z), jnp.logical_and(z == 0, at == last)))
+        def _():
+            for core in range(2):
+                pl.semaphore_signal(barrier, inc=1, device_id={"fs": 2 * at + core}, device_id_type=MESH)
+
+        return carry
+
+    lax.fori_loop(1, n_z, greet, 0)
 
     loads = [
         pltpu.make_async_copy(gain_hbm, gain, in_sem.at[0]),
@@ -132,11 +138,8 @@
             scale = lax.rsqrt(jnp.mean(values * values, axis=1, keepdims=True) + epsilon)
             normed[r : r + step_rows, :] = (values * scale).astype(jnp.bfloat16)
 
-    pl.semaphore_wait(barrier, planes + jnp.where(z > 1, 1, 0) + jnp.where(z == last, 1, 0))
-
-    @pl.when(jnp.logical_and(z > 0, z < last))
-    def _():
-        pl.semaphore_signal(barrier, inc=1, device_id={"fs": f + 2}, device_id_type=MESH)
+    lower = jnp.where(z > 0, 2 * (z - 1), 0) + jnp.where(z == last, 2, 0)
+    pl.semaphore_wait(barrier, planes + lower)
 
     @pl.when(z == last)
     def _():

time: 86.5 us -> 85.4 us (0.987)
  Pallas kernels: 83.1 us -> 82.1 us
    pallas_call x1, Pallas kernels: 83.1 us -> 82.1 us  [local(): pl.pallas_call(functools.partial(kernel, shards, planes), out_shape=(serv...]
where the time goes in v5:
time: 85.4 us; the launch traced here: 85.3 us
  Pallas kernels  82.1 us (96%)
  local copies, waits for them, and re-layouts  2.56 us (3%)
    pallas_call x1, Pallas kernels, local(): pl.pallas_call(functools.partial(kernel, shards, planes), out_shape=(serv...  82.1 us
    unnamed x5, local copies, waits for them, and re-layouts  2.56 us

profile of v5, /device:TPU:33, one launch (start us, length us, event | category | flops | bytes accessed | tf_op | source)
XLA Modules:
  0.0 85.3 jit_solution(14551642320207342990)
XLA Ops:
  0.6 82.1 %handoff.1 = (bf16[32,64,256]{2,1,0:T(8,128)(2,1)S(1)}, bf16[32,64,256]{2,1,0:T(8,128)(2,1)S(1)}, bf16[64,192]{1,0:T(8,128)(2,1)}) custom-call(bf16[192,2048]{1,0:T(8,128)(2,1)} %tok_hbm.1, f32[1,64]{1,0:T(1,128)} %bitcast.7, f32[64,2048]{1,0:T(8,128)} %up_hbm.1, f32[64,2048]{1,0:T(8,128)} %down_hbm.1), custom_call_target="tpu_custom_call" | custom-call | tf_op jit(solution)/shard_map/handoff/pallas_call | solution.py:456
  82.7 1.0 %copy.10 = bf16[2048,256]{1,0:T(8,128)(2,1)} copy(bf16[2048,256]{1,0:T(8,128)(2,1)S(1)} %bitcast.5) | data formatting | bytes 2097152
  83.7 0.0 copy-start
  83.7 1.0 %copy.11 = bf16[2048,256]{1,0:T(8,128)(2,1)} copy(bf16[2048,256]{1,0:T(8,128)(2,1)S(1)} %bitcast.4) | data formatting | bytes 2097152
  84.6 0.0 copy-done
  84.6 0.6 copy.12
Async XLA Ops:
  83.7 1.0 %copy-start = (bf16[64,192]{1,0:T(8,128)(2,1)S(1)}, bf16[64,192]{1,0:T(8,128)(2,1)}, u32[]{:S(2)}) copy-start(bf16[64,192]{1,0:T(8,128)(2,1)} %get-tuple-element.8) | copy-start | bytes 73732

commit v6 on v5

--- a/solution.py
+++ b/solution.py
@@ -9,7 +9,7 @@
 
 MESH = pl.DeviceIdType.MESH
 epsilon = 1e-06
-behind = 5.0
+behind = 8.0
 
 
 def ring_order(n):
@@ -455,7 +455,7 @@
     any_space = pl.BlockSpec(memory_space=pl.ANY)
     up, down, y = pl.pallas_call(
         functools.partial(kernel, shards, planes),
-        out_shape=(served, served, jax.ShapeDtypeStruct((rows, count), bf16)),
+        out_shape=(served, served, pltpu.VMEM((rows, count), bf16)),
         in_specs=[any_space] * 4,
         out_specs=(pl.BlockSpec(memory_space=pltpu.VMEM),) * 3,
         scratch_shapes=[

time: 85.4 us -> 83.6 us (0.979)
  Pallas kernels: 82.1 us -> 80.3 us
    pallas_call x1, Pallas kernels: 82.1 us -> 80.3 us  [local(): pl.pallas_call(functools.partial(kernel, shards, planes), out_shape=(serv...]
    unnamed x5 -> x3, local copies, waits for them, and re-layouts: 2.56 us -> 2.56 us
where the time goes in v6:
time: 83.6 us; the launch traced here: 83.5 us
  Pallas kernels  80.3 us (96%)
  local copies, waits for them, and re-layouts  2.56 us (3%)
    pallas_call x1, Pallas kernels, local(): pl.pallas_call(functools.partial(kernel, shards, planes), out_shape=(serv...  80.3 us
    unnamed x3, local copies, waits for them, and re-layouts  2.56 us

profile of v6, /device:TPU:33, one launch (start us, length us, event | category | flops | bytes accessed | tf_op | source)
XLA Modules:
  0.0 83.5 jit_solution(12168864340843642751)
XLA Ops:
  0.6 80.3 %handoff.1 = (bf16[32,64,256]{2,1,0:T(8,128)(2,1)S(1)}, bf16[32,64,256]{2,1,0:T(8,128)(2,1)S(1)}, bf16[64,192]{1,0:T(8,128)(2,1)S(1)}) custom-call(bf16[192,2048]{1,0:T(8,128)(2,1)} %tok_hbm.1, f32[1,64]{1,0:T(1,128)} %bitcast.7, f32[64,2048]{1,0:T(8,128)} %up_hbm.1, f32[64,2048]{1,0:T(8,128)} %down_hbm.1), custom_call_target="tpu_custom_call" | custom-call | tf_op jit(solution)/shard_map/handoff/pallas_call | solution.py:456
  80.9 1.0 %copy.10 = bf16[2048,256]{1,0:T(8,128)(2,1)} copy(bf16[2048,256]{1,0:T(8,128)(2,1)S(1)} %bitcast.5) | data formatting | bytes 2097152
  81.9 1.0 %copy.11 = bf16[2048,256]{1,0:T(8,128)(2,1)} copy(bf16[2048,256]{1,0:T(8,128)(2,1)S(1)} %bitcast.4) | data formatting | bytes 2097152
  82.9 0.6 copy.12

commit v7 on v6

--- a/solution.py
+++ b/solution.py
@@ -14,13 +14,13 @@
 
 def ring_order(n):
     half = n // 2
-    far = [d for d in range(half - 1, 3, -1)]
+    far = list(range(half - 1, 3, -2)) + list(range(half - 2, 3, -2))
     slots, first = [half], {half: 0}
     for d in far + [2, 1, 3]:
         first[d] = len(slots)
         slots += [d, n - d]
     slots.append(0)
-    return slots, first, 1 + 2 * len(far)
+    return slots, first, first[half - 2], 1 + 2 * len(far)
 
 
 def kernel(
@@ -300,7 +300,7 @@
 
     half = tok.shape[0] // 2
     low = lax.broadcasted_iota(jnp.int32, (half, 2 * rows), 1) < rows
-    slots, first, cut = ring_order(n_z)
+    slots, first, leaf, cut = ring_order(n_z)
 
     def part_of(slot):
         owner = around(z + slots[slot], n_z)
@@ -376,9 +376,10 @@
 
     def far_sums():
         from_across(1, far)
-        for slot in range(cut):
-            part_of(slot)
-        pair.append(exchange(0, 0, cut))
+        for j, (start, stop) in enumerate(((0, leaf), (leaf, cut))):
+            for slot in range(start, stop):
+                part_of(slot)
+            pair.append(exchange(j, start, stop))
 
     events = []
     for n in range(sources):
@@ -403,6 +404,7 @@
     for side, d, target in leaves:
         pass_on(side, d, target)
     from_across(1, close)
+    pair[1].wait_recv()
     settle(0, 6, (top_d, 7))
     settle(1, 6, (7,))
     pass_on(0, 6, 3)
@@ -413,7 +415,7 @@
     pass_on(1, 4, 3)
     for slot in range(cut, n_z):
         part_of(slot)
-    pair_near = exchange(1, cut, n_z)
+    pair_near = exchange(2, cut, n_z)
     pair_near.wait_recv()
     for d in (2, 1):
         for side in range(2):
@@ -477,8 +479,8 @@
             dma((2, shards)),
             dma((2, shards // planes * 5 // 4, 2)),
             dma((2, shards // planes * 5 // 4, 2)),
-            dma((2,)),
-            dma((2,)),
+            dma((3,)),
+            dma((3,)),
             dma((n_z,)),
             dma((n_z,)),
             pltpu.SemaphoreType.REGULAR,

time: 83.6 us -> 83.4 us (level)
  no operation moved by 1% of the time
where the time goes in v7:
time: 83.4 us; the launch traced here: 83.3 us
  Pallas kernels  80.1 us (96%)
  local copies, waits for them, and re-layouts  2.56 us (3%)
    pallas_call x1, Pallas kernels, local(): pl.pallas_call(functools.partial(kernel, shards, planes), out_shape=(serv...  80.1 us
    unnamed x3, local copies, waits for them, and re-layouts  2.56 us

profile of v7, /device:TPU:33, one launch (start us, length us, event | category | flops | bytes accessed | tf_op | source)
XLA Modules:
  0.0 83.3 jit_solution(15973683381572611533)
XLA Ops:
  0.6 80.1 %handoff.1 = (bf16[32,64,256]{2,1,0:T(8,128)(2,1)S(1)}, bf16[32,64,256]{2,1,0:T(8,128)(2,1)S(1)}, bf16[64,192]{1,0:T(8,128)(2,1)S(1)}) custom-call(bf16[192,2048]{1,0:T(8,128)(2,1)} %tok_hbm.1, f32[1,64]{1,0:T(1,128)} %bitcast.7, f32[64,2048]{1,0:T(8,128)} %up_hbm.1, f32[64,2048]{1,0:T(8,128)} %down_hbm.1), custom_call_target="tpu_custom_call" | custom-call | tf_op jit(solution)/shard_map/handoff/pallas_call | solution.py:458
  80.8 1.0 %copy.10 = bf16[2048,256]{1,0:T(8,128)(2,1)} copy(bf16[2048,256]{1,0:T(8,128)(2,1)S(1)} %bitcast.5) | data formatting | bytes 2097152
  81.7 1.0 %copy.11 = bf16[2048,256]{1,0:T(8,128)(2,1)} copy(bf16[2048,256]{1,0:T(8,128)(2,1)S(1)} %bitcast.4) | data formatting | bytes 2097152
  82.7 0.6 copy.12
